TPU v7x, 512 devices: a whole 4x4x16 slice. The times are simulated.
512 devices in a mesh: dp: 4 (over x), kv: 64 (over z, y), tp: 2 (over core).
Axes of the slice: x: 4, y: 4, z: 16, core: 2. Of those that a mesh axis runs over, the one named last changes fastest.
Arguments:
- tokens: bfloat16 [65536, 4096], P(('dp', 'kv')), parts along dimension 0, may hold values from -16 to 16
- query_weight: bfloat16 [4096, 1024], P('kv', 'tp'), may hold values from -0.09375 to 0.09375
- key_weight: bfloat16 [4096, 256], P('kv', 'tp'), may hold values from -0.09375 to 0.09375
- value_weight: bfloat16 [4096, 256], P('kv', 'tp'), may hold values from -0.09375 to 0.09375
- out_weight: bfloat16 [1024, 4096], P('kv', 'tp'), may hold values from -1.5 to 1.5
- chosen: int32 [2048, 16], P(('dp', 'kv')), parts along dimension 0, may hold values from -1 to 511, as said below
- live_length: int32 [4], P('dp'), parts along dimension 0, may hold values from 2048 to 16384
Outputs:
- mixed: bfloat16 [65536, 4096], P(('dp', 'kv'), 'tp'), parts along dimension 0
There are 4 independent parts, one for each index of `dp`. A program takes and returns all parts, laid end to end along the dimension named above; an argument that names none is the same for every part. Nothing has to cross between parts.
Inputs may be any that keep to these rules, and one draw needn't show every extreme that they name: `chosen`: row j lists 16 entries: entry 0 is j itself, the others are distinct blocks before j, or -1 for unused entries. The query blocks of one device together read at most 2 distinct blocks held by any one other device, and some device reads 2 of another's in every draw.
All inputs are finite; a program needn't handle non-finite values.
Results may differ from a plain program's by a relative error of at most 0.0085.
Values may be sent and summed in bfloat16 or wider, within the bound.
No kernel may reach another device: no remote copies, remote signals or barrier semaphores. Data moves between devices by JAX's collectives and lax.ppermute only.
A program may use at most 64 MiB of HBM per device.

v0:
```python
import jax
import jax.numpy as jnp
from jax import lax
from jax.sharding import Mesh
from jax.sharding import PartitionSpec as P

HD = 128
BLOCK = 32
CAP = 2
KV = ("kv_0", "kv_1")
DP_KV = ("dp", "kv_0", "kv_1")


def copy_for_each(shard, axis):
    count = lax.axis_size(axis)
    return lax.all_to_all(
        jnp.broadcast_to(shard[None], (count, *shard.shape)), axis, 0, 0, tiled=True
    )


def laid_out(blocks, dim):
    lengths = list(blocks.shape[1:])
    lengths[dim] *= blocks.shape[0]
    return jnp.moveaxis(blocks, 0, dim).reshape(lengths)


def gathered_copies(shard, axis, dim):
    blocks = copy_for_each(shard, axis)
    return laid_out(blocks, dim)


def spread_rows(shard):
    planes = lax.axis_size("dp")
    rows = shard.shape[0] // planes
    mine = lax.dynamic_slice_in_dim(shard, lax.axis_index("dp") * rows, rows, axis=0)
    column = copy_for_each(mine, "kv_0")
    every = copy_for_each(column, ("dp", "kv_1"))
    tall, wide = (column.shape[0], lax.axis_size("kv_1"))
    every = every.reshape(planes, wide, tall, rows, -1)
    return jnp.transpose(every, (2, 1, 0, 3, 4)).reshape(tall * wide * planes * rows, -1)


def body(tokens, query_weight, key_weight, value_weight, out_weight, chosen, live_length):
    rows = tokens.shape[0]
    per_dev = rows // BLOCK
    owners = lax.axis_size(KV)
    me = lax.axis_index(KV)

    def add_rows(piece):
        return jnp.dot(tokens, piece, preferred_element_type=jnp.float32)

    paired = add_rows(spread_rows(jnp.concatenate([key_weight, value_weight], axis=1))).astype(
        jnp.bfloat16
    )
    queries = add_rows(lax.all_gather(query_weight, KV, axis=0, tiled=True)).astype(jnp.bfloat16)
    width = paired.shape[1]
    local_blocks = paired.reshape(per_dev, BLOCK, width)
    valid = chosen >= 0
    safe = jnp.maximum(chosen, 0)
    blocks_all = owners * per_dev
    hits = (safe[:, :, None] == jnp.arange(blocks_all, dtype=jnp.int32)[None, None, :]) & valid[
        :, :, None
    ]
    needed = jnp.any(hits, axis=(0, 1)).reshape(owners, per_dev)
    needed = needed & (jnp.arange(owners, dtype=jnp.int32) != me)[:, None]
    ranks = jnp.cumsum(needed.astype(jnp.int32), axis=1)
    local_ids = jnp.arange(per_dev, dtype=jnp.int32)
    slot_lists = []
    for slot in range(CAP):
        marked = needed & (ranks == slot + 1)
        found = jnp.any(marked, axis=1)
        where_at = jnp.sum(jnp.where(marked, local_ids[None, :], 0), axis=1)
        slot_lists.append(jnp.where(found, where_at, -1))
    wanted = jnp.stack(slot_lists, axis=1)
    requested = lax.all_to_all(wanted, KV, split_axis=0, concat_axis=0, tiled=True)
    outgoing = local_blocks[jnp.maximum(requested, 0)]
    outgoing = jnp.where((requested >= 0)[:, :, None, None], outgoing, jnp.zeros((), jnp.bfloat16))
    incoming = lax.all_to_all(outgoing, KV, split_axis=0, concat_axis=0, tiled=True)
    table = jnp.concatenate([incoming.reshape(owners * CAP, BLOCK, width), local_blocks], axis=0)
    segment_retainer = safe // per_dev
    local_of = safe % per_dev
    match = (wanted[None, None, :, :] == local_of[:, :, None, None]) & (
        jnp.arange(owners, dtype=jnp.int32)[None, None, :, None]
        == segment_retainer[:, :, None, None]
    )
    slot_index = jnp.arange(owners * CAP, dtype=jnp.int32).reshape(owners, CAP)
    remote_at = jnp.sum(jnp.where(match, slot_index[None, None], 0), axis=(2, 3))
    position = jnp.where(segment_retainer == me, owners * CAP + local_of, remote_at)
    picked = table[position]
    near_keys = picked[..., :HD]
    near_values = picked[..., HD:]
    grouped = queries.reshape(per_dev, BLOCK, -1, HD)
    scores = jnp.einsum(
        "jqhd,jnbd->jhqnb", grouped, near_keys, preferred_element_type=jnp.float32
    ) * HD ** (-0.5)
    query_pos = (me * per_dev + jnp.arange(per_dev, dtype=jnp.int32))[:, None] * BLOCK + jnp.arange(
        BLOCK, dtype=jnp.int32
    )[None, :]
    key_pos = safe[:, :, None] * BLOCK + jnp.arange(BLOCK, dtype=jnp.int32)[None, None, :]
    allowed = valid[:, None, :, None] & (key_pos[:, None, :, :] <= query_pos[:, :, None, None])
    masked = jnp.where(allowed[:, None], scores, -jnp.inf)
    top = jnp.max(masked, axis=(3, 4), keepdims=True)
    weights = jnp.exp(masked - top)
    total = jnp.sum(weights, axis=(3, 4))
    summed = jnp.einsum(
        "jhqnb,jnbd->jqhd",
        weights.astype(jnp.bfloat16),
        near_values,
        preferred_element_type=jnp.float32,
    )
    result = summed / jnp.transpose(total, (0, 2, 1))[..., None]
    live = query_pos < live_length[0]
    result = jnp.where(live[:, :, None, None], result, 0.0)
    attended = result.astype(jnp.bfloat16).reshape(rows, -1)
    every_head = gathered_copies(attended, "tp", 1)
    mixed = jnp.dot(
        every_head,
        lax.all_gather(out_weight, KV, axis=0, tiled=True),
        preferred_element_type=jnp.float32,
    )
    return mixed.astype(jnp.bfloat16)


def solution(mesh):
    split = Mesh(
        mesh.devices.reshape(mesh.shape["dp"], 16, 4, mesh.shape["tp"]),
        ("dp", "kv_0", "kv_1", "tp"),
    )
    placed = (
        P(DP_KV, None),
        P(KV, "tp"),
        P(KV, "tp"),
        P(KV, "tp"),
        P(KV, "tp"),
        P(DP_KV, None),
        P("dp"),
    )
    return jax.shard_map(
        body, mesh=split, in_specs=placed, out_specs=P(DP_KV, "tp"), check_vma=False
    )
```

profile of v0, /device:TPU:2, one launch (start us, length us, event | category | flops | bytes accessed | tf_op | source)
XLA Modules:
  0.0 375.7 jit_solution(15250901952565097661)
XLA Ops:
  6.5 0.7 all-gather.3.cloned.1.call-update
  7.3 0.7 broadcast_compare_fusion.1
  8.0 0.7 add_select_fusion.1
  8.7 0.1 fusion.21
  8.8 0.1 reshape.152
  8.9 0.1 and_convert_fusion
  9.0 0.2 reduce_window_sum.11
  9.1 0.2 select_reduce_fusion.2
  9.3 0.1 reduce_or.28
  9.4 0.1 reduce_or.29
  9.6 0.7 copy.37
  10.3 18.7 %all-to-all-start = ((s32[64,1,2]{2,1,0:T(1,128)}), s32[64,1,2]{2,1,0:T(1,128)S(1)}, u32[]{:S(2)}, u32[]{:S(2)}) async-start(s32[64,1,2]{2,1,0:T(1,128)} %copy.37), calls=%async_computation | async-start | bytes 65536 | tf_op jit(solution)/shard_map/all_to_all | solution.py:75
  29.1 0.7 fusion.22
  29.8 13.8 %all-to-all-done = s32[64,1,2]{2,1,0:T(1,128)S(1)} async-done(((s32[64,1,2]{2,1,0:T(1,128)}), s32[64,1,2]{2,1,0:T(1,128)S(1)}, u32[]{:S(2)}, u32[]{:S(2)}) %all-to-all-start) | async-done | bytes 544 | tf_op jit(solution)/shard_map/all_to_all | solution.py:75
  43.6 16.8 %all_to_all.29 = bf16[16,16,256]{2,1,0:T(8,128)(2,1)S(1)} all-to-all(bf16[16,16,256]{2,1,0:T(8,128)(2,1)S(1)} %broadcast_in_dim.122), channel_id=1, replica_groups=mesh['dp'=4,'kv_0'=16,'kv_1'=4,'tp'=2] {'kv_0'}, dimensions={0} | all-to-all | bytes 262144 | tf_op jit(solution)/shard_map/all_to_all | solution.py:16
  60.4 1.5 broadcast_in_dim.123
  61.9 5.4 %all-to-all-start.2 = ((bf16[16,16,16,256]{3,2,1,0:T(8,128)(2,1)}), bf16[16,16,16,256]{3,2,1,0:T(8,128)(2,1)}, u32[]{:S(2)}, u32[]{:S(2)}) async-start(bf16[16,16,16,256]{3,2,1,0:T(8,128)(2,1)} %broadcast_in_dim.123), calls=%async_computation.2 | async-start | bytes 4194304 | tf_op jit(solution)/shard_map/all_to_all | solution.py:16
  67.3 0.1 maximum_reduce_fusion
  67.4 0.1 reshape.161
  67.6 0.1 copy.38
  67.7 0.1 copy.39
  67.9 24.0 %all-to-all-done.2 = bf16[16,16,16,256]{3,2,1,0:T(8,128)(2,1)} async-done(((bf16[16,16,16,256]{3,2,1,0:T(8,128)(2,1)}), bf16[16,16,16,256]{3,2,1,0:T(8,128)(2,1)}, u32[]{:S(2)}, u32[]{:S(2)}) %all-to-all-start.2) | async-done | bytes 2097184 | tf_op jit(solution)/shard_map/all_to_all | solution.py:16
  91.9 1.9 copy.40
  93.8 0.7 convolution_convert_fusion.2
  94.5 2.0 gather_fusion
  96.5 3.1 broadcast_select_fusion
  99.6 8.6 %all-to-all-start.3 = ((bf16[64,2,32,256]{3,2,1,0:T(8,128)(2,1)}), bf16[64,2,32,256]{3,2,1,0:T(8,128)(2,1)}, u32[]{:S(2)}, u32[]{:S(2)}) async-start(bf16[64,2,32,256]{3,2,1,0:T(8,128)(2,1)} %broadcast_select_fusion), calls=%async_computation.3 | async-start | bytes 4194304 | tf_op jit(solution)/shard_map/all_to_all | solution.py:78
  108.2 0.7 all-gather.5.cloned.1.call-update
  109.0 0.1 iota_compare_fusion.1
  109.0 0.3 select_reduce_fusion
  109.4 0.1 reshape.169
  110.1 0.1 broadcast_compare_fusion.2
  110.3 0.1 iota_add_fusion
  110.4 1.0 compare_and_fusion
  111.4 105.0 %all-gather.3.cloned.1.call-done = bf16[4096,512]{1,0:T(8,128)(2,1)} async-done(((bf16[64,512]{1,0:T(8,128)(2,1)}), bf16[4096,512]{1,0:T(8,128)(2,1)}) %all-gather.3.cloned.1.call-update) | async-done | bytes 4194320 | tf_op jit(solution)/shard_map/all_gather | solution.py:55
  216.4 3.4 convolution_convert_fusion.1
  219.9 6.6 %all-to-all-done.3 = bf16[64,2,32,256]{3,2,1,0:T(8,128)(2,1)} async-done(((bf16[64,2,32,256]{3,2,1,0:T(8,128)(2,1)}), bf16[64,2,32,256]{3,2,1,0:T(8,128)(2,1)}, u32[]{:S(2)}, u32[]{:S(2)}) %all-to-all-start.3) | async-done | bytes 2097184 | tf_op jit(solution)/shard_map/all_to_all | solution.py:78
  226.6 3.2 pad_maximum_fusion
  229.7 3.7 gather_fusion.1
  233.4 2.9 fusion.2
  236.4 2.5 fusion
  238.9 2.2 fusion.16
  241.1 0.1 copy.43
  241.3 0.1 copy.44
  241.4 0.8 broadcast_in_dim.132
  242.3 3.5 all-to-all-start.4
  245.8 118.7 %all-gather.5.cloned.1.call-done = bf16[1024,2048]{1,0:T(8,128)(2,1)} async-done(((bf16[16,2048]{1,0:T(8,128)(2,1)}), bf16[1024,2048]{1,0:T(8,128)(2,1)}) %all-gather.5.cloned.1.call-update) | async-done | bytes 4194320 | tf_op jit(solution)/shard_map/all_gather | solution.py:118
  364.4 4.4 %convolution_convert_fusion = bf16[256,2048]{1,0:T(8,128)(2,1)} fusion(bf16[256,1024]{0,1:T(8,128)(2,1)S(1)} %bitcast.93, bf16[1024,2048]{1,0:T(8,128)(2,1)} %all-gather.5.cloned.1.call-done), kind=kOutput, calls=%fused_computation.9 | convolution fusion | flops 1074266112 | bytes 5767168 | tf_op jit(solution)/shard_map/dot_general | solution.py:116
  (22 shorter events, 0.3 us)
Async XLA Ops:
  6.5 87.2 %copy-start = (bf16[256,4096]{1,0:T(8,128)(2,1)S(1)}, bf16[256,4096]{1,0:T(8,128)(2,1)}, u32[]{:S(2)}) copy-start(bf16[256,4096]{1,0:T(8,128)(2,1)} %param.7) | copy-start | bytes 6291460
  6.5 209.9 %all-gather.3.cloned.1.call-start = ((), (), s32[]{:S(2)}) async-start(), calls=%async_computation.5 | async-start | bytes 4259840 | tf_op jit(solution)/shard_map/all_gather | solution.py:55
  10.3 33.3 %all-to-all-start = ((s32[64,1,2]{2,1,0:T(1,128)}), s32[64,1,2]{2,1,0:T(1,128)S(1)}, u32[]{:S(2)}, u32[]{:S(2)}) async-start(s32[64,1,2]{2,1,0:T(1,128)} %copy.37), calls=%async_computation | async-start | bytes 65536 | tf_op jit(solution)/shard_map/all_to_all | solution.py:75
  61.9 29.9 %all-to-all-start.2 = ((bf16[16,16,16,256]{3,2,1,0:T(8,128)(2,1)}), bf16[16,16,16,256]{3,2,1,0:T(8,128)(2,1)}, u32[]{:S(2)}, u32[]{:S(2)}) async-start(bf16[16,16,16,256]{3,2,1,0:T(8,128)(2,1)} %broadcast_in_dim.123), calls=%async_computation.2 | async-start | bytes 4194304 | tf_op jit(solution)/shard_map/all_to_all | solution.py:16
  99.6 9.7 %copy-start.2 = (s32[8,16]{1,0:T(8,128)S(1)}, s32[8,16]{1,0:T(8,128)}, u32[]{:S(2)}) copy-start(s32[8,16]{1,0:T(8,128)} %param.12) | copy-start | bytes 1540
  99.6 126.9 %all-to-all-start.3 = ((bf16[64,2,32,256]{3,2,1,0:T(8,128)(2,1)}), bf16[64,2,32,256]{3,2,1,0:T(8,128)(2,1)}, u32[]{:S(2)}, u32[]{:S(2)}) async-start(bf16[64,2,32,256]{3,2,1,0:T(8,128)(2,1)} %broadcast_select_fusion), calls=%async_computation.3 | async-start | bytes 4194304 | tf_op jit(solution)/shard_map/all_to_all | solution.py:78
  108.2 256.2 %all-gather.5.cloned.1.call-start = ((), (), s32[]{:S(2)}) async-start(), calls=%async_computation.6 | async-start | bytes 4259840 | tf_op jit(solution)/shard_map/all_gather | solution.py:118
  236.3 2.6 copy-start.1
  242.3 122.2 %all-to-all-start.4 = ((bf16[2,256,512]{1,2,0:T(8,128)(2,1)}), bf16[2,256,512]{1,2,0:T(8,128)(2,1)S(1)}, u32[]{:S(2)}, u32[]{:S(2)}) async-start(bf16[2,256,512]{1,2,0:T(8,128)(2,1)} %broadcast_in_dim.132), calls=%async_computation.4 | async-start | bytes 1048576 | tf_op jit(solution)/shard_map/all_to_all | solution.py:16
Sparse Core Ops, SparseCore 0:
  10.3 206.0 all-gather.2
  219.4 145.0 all-gather.4
where the time goes:
time: 376 us
  waiting for transfers between devices  270 us (72%)
  starting transfers between devices  36.2 us (10%)
  blocking collectives  16.8 us (4%)
  between operations  14.3 us (4%)
  matrix products  13.7 us (4%)
  other arithmetic  13.5 us (4%)
  local copies, waits for them, and re-layouts  11.6 us (3%)
    all_gather x1, waiting for transfers between devices, body(): lax.all_gather(out_weight, KV, axis=0, tiled=True)  119 us
    all_gather x1, waiting for transfers between devices, body(): lax.all_gather(query_weight, KV, axis=0, tiled=True)  105 us
    all_to_all x2, waiting for transfers between devices, copy_for_each(): lax.all_to_all(jnp.broadcast_to(shard[None], (count, *shard.shape)), axis...  24 us
    all_to_all x1, starting transfers between devices, body(): lax.all_to_all(wanted, KV, split_axis=0, concat_axis=0, tiled=True)  18.7 us
    all_to_all x1, blocking collectives, copy_for_each(): lax.all_to_all(jnp.broadcast_to(shard[None], (count, *shard.shape)), axis...  16.8 us
    all_to_all x1, waiting for transfers between devices, body(): lax.all_to_all(wanted, KV, split_axis=0, concat_axis=0, tiled=True)  13.8 us
    all_to_all x2, starting transfers between devices, copy_for_each(): lax.all_to_all(jnp.broadcast_to(shard[None], (count, *shard.shape)), axis...  8.91 us
    all_to_all x1, starting transfers between devices, body(): lax.all_to_all(outgoing, KV, split_axis=0, concat_axis=0, tiled=True)  8.55 us
  transfers between devices with their start and end apart: 6, of which 5 were waited for; matrix products, arithmetic and copies ran while one was open for 9% of the time, Pallas kernels for 0%

commit v1 on v0

--- a/solution.py
+++ b/solution.py
@@ -115,7 +115,9 @@
     every_head = gathered_copies(attended, "tp", 1)
     mixed = jnp.dot(
         every_head,
-        lax.all_gather(out_weight, KV, axis=0, tiled=True),
+        jnp.concatenate(
+            lax.all_to_all(jnp.stack([out_weight] * lax.axis_size(KV)), KV, 0, 0), axis=0
+        ),
         preferred_element_type=jnp.float32,
     )
     return mixed.astype(jnp.bfloat16)

time: 376 us -> 475 us (1.26)
  blocking collectives: 16.8 us -> 222 us
  waiting for transfers between devices: 270 us -> 169 us
    all_to_all x0 -> x1, blocking collectives: none -> 201 us  [body(): lax.all_to_all(jnp.stack([out_weight] * lax.axis_size(KV)), KV, 0, 0)]
    all_gather x1 -> x0, waiting for transfers between devices: 119 us -> none  [body(): lax.all_gather(out_weight, KV, axis=0, tiled=True)]
    all_gather x1, waiting for transfers between devices: 105 us -> 131 us  [body(): lax.all_gather(query_weight, KV, axis=0, tiled=True)]
    all_to_all x1, waiting for transfers between devices: 6.65 us -> 0.01 us  [body(): lax.all_to_all(outgoing, KV, split_axis=0, concat_axis=0, tiled=True)]
    all_to_all x1 -> x2, blocking collectives: 16.8 us -> 20.6 us  [copy_for_each(): lax.all_to_all(jnp.broadcast_to(shard[None], (count, *shard.shape)), axis...]
    all_to_all x2 -> x1, waiting for transfers between devices: 24 us -> 23.4 us  [copy_for_each(): lax.all_to_all(jnp.broadcast_to(shard[None], (count, *shard.shape)), axis...]
  transfers between devices with their start and end apart: 6 -> 4, of which waited for: 5 -> 3; matrix products, arithmetic and copies ran while one was open for 9% -> 3% of each run, Pallas kernels for 0% -> 0%
where the time goes in v1:
time: 475 us; the launch traced here: 474 us
  blocking collectives  222 us (47%)
  waiting for transfers between devices  169 us (36%)
  starting transfers between devices  32 us (7%)
  between operations  14.3 us (3%)
  other arithmetic  13.7 us (3%)
  matrix products  11.5 us (2%)
  local copies, waits for them, and re-layouts  11.2 us (2%)
    all_to_all x1, blocking collectives, body(): lax.all_to_all(jnp.stack([out_weight] * lax.axis_size(KV)), KV, 0, 0)  201 us
    all_gather x1, waiting for transfers between devices, body(): lax.all_gather(query_weight, KV, axis=0, tiled=True)  131 us
    all_to_all x1, waiting for transfers between devices, copy_for_each(): lax.all_to_all(jnp.broadcast_to(shard[None], (count, *shard.shape)), axis...  23.4 us
    all_to_all x2, blocking collectives, copy_for_each(): lax.all_to_all(jnp.broadcast_to(shard[None], (count, *shard.shape)), axis...  20.6 us
    all_to_all x1, starting transfers between devices, body(): lax.all_to_all(wanted, KV, split_axis=0, concat_axis=0, tiled=True)  18.7 us
    all_to_all x1, waiting for transfers between devices, body(): lax.all_to_all(wanted, KV, split_axis=0, concat_axis=0, tiled=True)  13.8 us
  transfers between devices with their start and end apart: 4, of which 3 were waited for; matrix products, arithmetic and copies ran while one was open for 3% of the time, Pallas kernels for 0%

profile of v1, /device:TPU:2, one launch (start us, length us, event | category | flops | bytes accessed | tf_op | source)
XLA Modules:
  0.0 474.0 jit_solution(7029808317829402585)
XLA Ops:
  6.5 0.8 add_select_fusion.1
  7.4 0.7 broadcast_compare_fusion.1
  8.1 0.1 fusion.21
  8.2 0.1 reshape.157
  8.3 0.1 and_convert_fusion
  8.4 0.2 reduce_window_sum.11
  8.5 0.2 select_reduce_fusion.2
  8.7 0.1 reduce_or.28
  8.9 0.1 reduce_or.29
  9.0 0.7 copy.37
  9.7 18.7 %all-to-all-start = ((s32[64,1,2]{2,1,0:T(1,128)}), s32[64,1,2]{2,1,0:T(1,128)S(1)}, u32[]{:S(2)}, u32[]{:S(2)}) async-start(s32[64,1,2]{2,1,0:T(1,128)} %copy.37), calls=%async_computation | async-start | bytes 65536 | tf_op jit(solution)/shard_map/all_to_all | solution.py:75
  28.5 0.7 fusion.22
  29.2 13.8 %all-to-all-done = s32[64,1,2]{2,1,0:T(1,128)S(1)} async-done(((s32[64,1,2]{2,1,0:T(1,128)}), s32[64,1,2]{2,1,0:T(1,128)S(1)}, u32[]{:S(2)}, u32[]{:S(2)}) %all-to-all-start) | async-done | bytes 544 | tf_op jit(solution)/shard_map/all_to_all | solution.py:75
  43.0 16.5 %all_to_all.34 = bf16[16,16,256]{2,1,0:T(8,128)(2,1)S(1)} all-to-all(bf16[16,16,256]{2,1,0:T(8,128)(2,1)S(1)} %broadcast_in_dim.122), channel_id=1, replica_groups=mesh['dp'=4,'kv_0'=16,'kv_1'=4,'tp'=2] {'kv_0'}, dimensions={0} | all-to-all | bytes 262144 | tf_op jit(solution)/shard_map/all_to_all | solution.py:16
  59.5 1.5 broadcast_in_dim.123
  61.1 5.7 %all-to-all-start.2 = ((bf16[16,16,16,256]{3,2,1,0:T(8,128)(2,1)}), bf16[16,16,16,256]{3,2,1,0:T(8,128)(2,1)}, u32[]{:S(2)}, u32[]{:S(2)}) async-start(bf16[16,16,16,256]{3,2,1,0:T(8,128)(2,1)} %broadcast_in_dim.123), calls=%async_computation.2 | async-start | bytes 4194304 | tf_op jit(solution)/shard_map/all_to_all | solution.py:16
  66.8 0.7 all-gather.2.cloned.1.call-update
  67.5 0.1 maximum_reduce_fusion
  67.6 0.1 reshape.167
  67.8 0.1 copy.38
  67.9 0.1 copy.39
  68.0 23.4 %all-to-all-done.2 = bf16[16,16,16,256]{3,2,1,0:T(8,128)(2,1)} async-done(((bf16[16,16,16,256]{3,2,1,0:T(8,128)(2,1)}), bf16[16,16,16,256]{3,2,1,0:T(8,128)(2,1)}, u32[]{:S(2)}, u32[]{:S(2)}) %all-to-all-start.2) | async-done | bytes 2097184 | tf_op jit(solution)/shard_map/all_to_all | solution.py:16
  91.4 1.9 copy.40
  93.3 0.7 convolution_convert_fusion.2
  94.1 2.0 gather_fusion
  96.1 3.2 broadcast_select_fusion
  99.3 7.5 %all-to-all-start.3 = ((bf16[64,2,32,256]{3,2,1,0:T(8,128)(2,1)}), bf16[64,2,32,256]{3,2,1,0:T(8,128)(2,1)}, u32[]{:S(2)}, u32[]{:S(2)}) async-start(bf16[64,2,32,256]{3,2,1,0:T(8,128)(2,1)} %broadcast_select_fusion), calls=%async_computation.3 | async-start | bytes 4194304 | tf_op jit(solution)/shard_map/all_to_all | solution.py:78
  106.8 0.1 iota_compare_fusion.1
  106.9 0.3 select_reduce_fusion
  107.3 0.1 reshape.175
  108.0 0.1 broadcast_compare_fusion.2
  108.1 0.1 iota_add_fusion.1
  108.2 0.1 iota_add_fusion
  108.2 1.0 compare_and_fusion
  109.3 131.2 %all-gather.2.cloned.1.call-done = bf16[4096,512]{1,0:T(8,128)(2,1)} async-done(((bf16[64,512]{1,0:T(8,128)(2,1)}), bf16[4096,512]{1,0:T(8,128)(2,1)}) %all-gather.2.cloned.1.call-update) | async-done | bytes 4194320 | tf_op jit(solution)/shard_map/all_gather | solution.py:55
  240.5 3.4 convolution_convert_fusion.1
  243.9 0.1 reshape.162
  244.0 3.2 pad_maximum_fusion
  247.2 3.6 gather_fusion.1
  250.8 2.9 fusion.2
  253.7 2.5 fusion
  256.2 2.2 fusion.16
  258.4 0.1 copy.43
  258.6 0.1 copy.44
  258.8 4.2 all_to_all.35
  263.0 0.5 stack.5
  263.5 201.4 %all_to_all.36 = bf16[64,16,2048]{2,1,0:T(8,128)(2,1)S(1)} all-to-all(bf16[64,16,2048]{2,1,0:T(8,128)(2,1)S(1)} %stack.5), channel_id=1, replica_groups=mesh['dp'=4,'kv_0'=16,'kv_1'=4,'tp'=2] {'kv_0','kv_1'}, dimensions={0} | all-to-all | bytes 8388608 | tf_op jit(solution)/shard_map/all_to_all | solution.py:119
  464.9 2.2 convolution_convert_fusion
  (22 shorter events, 0.2 us)
Async XLA Ops:
  6.5 86.8 %copy-start = (bf16[256,4096]{1,0:T(8,128)(2,1)S(1)}, bf16[256,4096]{1,0:T(8,128)(2,1)}, u32[]{:S(2)}) copy-start(bf16[256,4096]{1,0:T(8,128)(2,1)} %param.7) | copy-start | bytes 6291460
  9.7 33.3 %all-to-all-start = ((s32[64,1,2]{2,1,0:T(1,128)}), s32[64,1,2]{2,1,0:T(1,128)S(1)}, u32[]{:S(2)}, u32[]{:S(2)}) async-start(s32[64,1,2]{2,1,0:T(1,128)} %copy.37), calls=%async_computation | async-start | bytes 65536 | tf_op jit(solution)/shard_map/all_to_all | solution.py:75
  61.1 30.4 %all-to-all-start.2 = ((bf16[16,16,16,256]{3,2,1,0:T(8,128)(2,1)}), bf16[16,16,16,256]{3,2,1,0:T(8,128)(2,1)}, u32[]{:S(2)}, u32[]{:S(2)}) async-start(bf16[16,16,16,256]{3,2,1,0:T(8,128)(2,1)} %broadcast_in_dim.123), calls=%async_computation.2 | async-start | bytes 4194304 | tf_op jit(solution)/shard_map/all_to_all | solution.py:16
  66.7 173.7 %all-gather.2.cloned.1.call-start = ((), (), s32[]{:S(2)}) async-start(), calls=%async_computation.6 | async-start | bytes 4259840 | tf_op jit(solution)/shard_map/all_gather | solution.py:55
  99.3 8.0 %copy-start.3 = (s32[8,16]{1,0:T(8,128)S(1)}, s32[8,16]{1,0:T(8,128)}, u32[]{:S(2)}) copy-start(s32[8,16]{1,0:T(8,128)} %param.12) | copy-start | bytes 1540
  99.3 144.7 %all-to-all-start.3 = ((bf16[64,2,32,256]{3,2,1,0:T(8,128)(2,1)}), bf16[64,2,32,256]{3,2,1,0:T(8,128)(2,1)}, u32[]{:S(2)}, u32[]{:S(2)}) async-start(bf16[64,2,32,256]{3,2,1,0:T(8,128)(2,1)} %broadcast_select_fusion), calls=%async_computation.3 | async-start | bytes 4194304 | tf_op jit(solution)/shard_map/all_to_all | solution.py:78
  253.7 2.6 copy-start.1
  258.4 4.5 copy-start.2
Sparse Core Ops, SparseCore 0:
  70.5 169.9 all-gather.1
